TPU v7x, 32 devices: a whole 2x2x4 slice. The times are simulated.
32 devices in a mesh: grp: 2 (over x), tp: 16 (over z, y, core).
Axes of the slice: x: 2, y: 2, z: 4, core: 2. Of those that a mesh axis runs over, the one named last changes fastest.
Arguments:
- tokens: bfloat16 [3072, 2048], P('grp', 'tp'), parts along dimension 0, may hold values from -6 to 6
- lengths: int32 [192], P('grp'), parts along dimension 0, may hold values from 1 to 16, 960 in all
- gain_first: float32 [2048], replicated, may hold values from 0.1 to 1.9
- query_first: bfloat16 [2048, 1024], P(None, 'tp'), may hold values from -0.125 to 0.125
- key_first: bfloat16 [2048, 1024], P(None, 'tp'), may hold values from -0.125 to 0.125
- value_first: bfloat16 [2048, 2048], P(None, 'tp'), may hold values from -0.125 to 0.125
- gate_first: bfloat16 [2048, 2048], P(None, 'tp'), may hold values from -0.125 to 0.125
- out_first: bfloat16 [2048, 2048], P('tp'), may hold values from -0.1875 to 0.1875
- state_first: float32 [192, 16, 64, 128], P('grp', 'tp'), parts along dimension 0, may hold values from -0.9 to 0.9
- gain_second: float32 [2048], replicated, may hold values from 0.1 to 1.9
- query_second: bfloat16 [2048, 1024], P(None, 'tp'), may hold values from -0.125 to 0.125
- key_second: bfloat16 [2048, 1024], P(None, 'tp'), may hold values from -0.125 to 0.125
- value_second: bfloat16 [2048, 2048], P(None, 'tp'), may hold values from -0.125 to 0.125
- gate_second: bfloat16 [2048, 2048], P(None, 'tp'), may hold values from -0.125 to 0.125
- out_second: bfloat16 [2048, 2048], P('tp'), may hold values from -0.1875 to 0.1875
- state_second: float32 [192, 16, 64, 128], P('grp', 'tp'), parts along dimension 0, may hold values from -0.9 to 0.9
Outputs:
- mixed_out: bfloat16 [3072, 2048], P('grp', 'tp'), parts along dimension 0
- state_first_new: float32 [192, 16, 64, 128], P('grp', 'tp'), parts along dimension 0
- state_second_new: float32 [192, 16, 64, 128], P('grp', 'tp'), parts along dimension 0
There are 2 independent parts, one for each index of `grp`. A program takes and returns all parts, laid end to end along the dimension named above; an argument that names none is the same for every part. Nothing has to cross between parts.
All inputs are finite; a program needn't handle non-finite values.
Results may differ from a plain program's by a relative error of at most 0.025.
Values may be sent and summed in bfloat16 or wider, within the bound.
A program may use at most 128 MiB of HBM per device.

v0:
```python
import functools

import jax
import jax.numpy as jnp
from jax import lax
from jax.experimental import pallas as pl
from jax.experimental.pallas import tpu as pltpu
from jax.sharding import PartitionSpec as P

PAST_LEN = 16384
LIVE_TOTAL = 960

NORM_EPSILON = 1e-06
ROPE_BASE = 10000.0

MESH = pl.DeviceIdType.MESH
F32 = jnp.float32
BF16 = jnp.bfloat16


def decay_logs(head_count):
    head_total = lax.axis_size("tp") * head_count
    head_ids = (lax.axis_index("tp") * head_count + jnp.arange(head_count)).astype(F32)
    return jnp.log(1.0 - 2.0 ** (-1.5 - 6.0 * head_ids / (head_total - 1)))


def rope_tables(block_len, key_dim):
    half_dim = key_dim // 2
    inverse = ROPE_BASE ** (-jnp.arange(half_dim, dtype=F32) / half_dim)
    positions = PAST_LEN + jnp.arange(block_len, dtype=F32)
    angles = positions[:, None] * inverse[None, :]
    cosines, sines = jnp.cos(angles), jnp.sin(angles)
    cosines = jnp.concatenate([cosines, cosines], axis=1)
    sines = jnp.concatenate([-sines, sines], axis=1)
    scale = key_dim ** (-0.5)
    return jnp.concatenate([cosines, cosines * scale, sines, sines * scale], axis=1)


def retain(qkv, lengths, state_in):
    batch_size, head_count, key_dim, value_dim = state_in.shape
    block_len = qkv.shape[0] // batch_size
    log_gamma = decay_logs(head_count)
    queries = qkv[:, :key_dim].reshape(batch_size, block_len, 1, key_dim)
    key_rows = qkv[:, key_dim : 2 * key_dim].reshape(batch_size, block_len, 1, key_dim)
    values = qkv[:, 2 * key_dim :].reshape(batch_size, block_len, 1, value_dim)
    slot_ids = jnp.arange(block_len).astype(F32)
    live_count = lengths.astype(F32)
    active = (slot_ids[None, :] < live_count[:, None]).astype(F32)
    step_gap = slot_ids[:, None] - slot_ids[None, :]
    causal = (step_gap >= 0.0).astype(F32)
    within = jnp.exp(log_gamma[:, None, None] * jnp.maximum(step_gap, 0.0)[None]) * causal[None]
    scores = jnp.einsum("bihd,bjhd->bhij", queries, key_rows, preferred_element_type=F32)
    weights = (scores * within[None]).astype(BF16)
    inner_part = jnp.einsum("bhij,bjhe->bihe", weights, values, preferred_element_type=F32)
    carried = jnp.einsum(
        "bihd,bhde->bihe", queries.astype(F32), state_in, precision=lax.Precision.HIGHEST
    )
    carried = (
        carried * jnp.exp(log_gamma[None, None, :] * (slot_ids[None, :, None] + 1.0))[..., None]
    )
    retained = (inner_part + carried) * active[:, :, None, None]
    lead_gap = live_count[:, None] - 1.0 - slot_ids[None, :]
    key_weight = (
        jnp.exp(log_gamma[None, None, :] * jnp.maximum(lead_gap, 0.0)[:, :, None])
        * active[:, :, None]
    )
    added_state = jnp.einsum(
        "bjhd,bjhe->bhde",
        key_rows.astype(F32) * key_weight[..., None],
        values.astype(F32),
        precision=lax.Precision.HIGHEST,
    )
    new_state = (
        state_in * jnp.exp(log_gamma[None, :] * live_count[:, None])[:, :, None, None] + added_state
    )
    inv_rms = lax.rsqrt(jnp.mean(retained * retained, axis=-1, keepdims=True) + NORM_EPSILON)
    normed = (retained * inv_rms).astype(BF16)
    return normed.reshape(batch_size * block_len, value_dim), new_state


def retention_kernel(key_dim, block_len, *refs):
    decay, side_ref, row_ref, within_ref, qkv_ref, gate_ref, state_ref = refs[:7]
    h_ref, new_ref, total = refs[7:]
    i = pl.program_id(0)
    rows = qkv_ref.shape[0]
    both = 2 * key_dim
    size = side_ref.shape[0]
    group = size // block_len
    side = side_ref[...]

    slots = lax.broadcasted_iota(jnp.int32, (size, rows), 1)
    hot = jnp.where(slots == side[:, 0:1].astype(jnp.int32), 1.0, 0.0).astype(BF16)
    padded = jnp.dot(hot, qkv_ref[...], preferred_element_type=F32)
    qk, values = padded[:, :both], padded[:, both:].astype(BF16)
    front = lax.broadcasted_iota(jnp.int32, qk.shape, 1) < key_dim
    turned = pltpu.roll(qk, key_dim, 1)
    queries, keys = jnp.where(front, qk, turned), jnp.where(front, turned, qk)
    scores = lax.dot_general(
        jnp.where(front, qk, 0.0).astype(BF16),
        keys.astype(BF16),
        (((1,), (1,)), ((), ())),
        preferred_element_type=F32,
    )
    weights = (scores * within_ref[...]).astype(BF16)
    retained = jnp.dot(weights, values, preferred_element_type=F32)

    wide = (size, group * key_dim)
    own = lax.div(lax.broadcasted_iota(jnp.int32, wide, 0), block_len) == lax.div(
        lax.broadcasted_iota(jnp.int32, wide, 1), key_dim
    )

    def per_sequence(doubled):
        spread = jnp.concatenate([doubled] * (group // 2), axis=1)
        return jnp.where(own, spread, 0.0).astype(BF16)

    state = state_ref[...].reshape(group * key_dim, state_ref.shape[-1])
    high = state.astype(BF16)
    low = (state - high.astype(F32)).astype(BF16)
    wide_q = per_sequence(queries)
    carried = jnp.dot(wide_q, high, preferred_element_type=F32)
    carried = carried + jnp.dot(wide_q, low, preferred_element_type=F32)
    retained = retained + carried * side[:, 1:2]
    inv = lax.rsqrt(jnp.mean(retained * retained, axis=-1, keepdims=True) + NORM_EPSILON)
    normed = (retained * inv).astype(BF16)
    places = lax.broadcasted_iota(jnp.int32, (rows, size), 0)
    back = jnp.where(places == row_ref[...], 1.0, 0.0).astype(BF16)
    part = jnp.dot(back, normed, preferred_element_type=F32)

    @pl.when(i == 0)
    def _():
        total[...] = part

    @pl.when(i > 0)
    def _():
        total[...] += part

    scaled = keys * side[:, 2:3]
    k_high = scaled.astype(BF16).astype(F32)
    added = None
    for piece in (k_high, scaled - k_high):
        term = lax.dot_general(
            per_sequence(piece), values, (((0,), (0,)), ((), ())), preferred_element_type=F32
        )
        added = term if added is None else added + term
    for b in range(group):
        new_ref[b] = (
            state_ref[b] * decay[i * group + b] + added[b * key_dim : (b + 1) * key_dim, :]
        )

    @pl.when(i == pl.num_programs(0) - 1)
    def _():
        h_ref[...] = (total[...] * gate_ref[...]).astype(BF16)


def retain_packed(decay, side, row, within, qkv, gate, state, block_len):
    batch_size, _, key_dim, value_dim = state.shape
    rows = qkv.shape[0]
    size = within.shape[0]
    group = size // block_len
    whole = lambda *shape: pl.BlockSpec(shape, lambda i: (0,) * len(shape))
    state_spec = pl.BlockSpec((group, key_dim, value_dim), lambda i: (i, 0, 0))
    h, new_state = pl.pallas_call(
        functools.partial(retention_kernel, key_dim, block_len),
        grid=(batch_size // group,),
        out_shape=[
            jax.ShapeDtypeStruct((rows, value_dim), BF16),
            jax.ShapeDtypeStruct((batch_size, key_dim, value_dim), F32),
        ],
        in_specs=[
            pl.BlockSpec(memory_space=pltpu.SMEM),
            pl.BlockSpec((size, side.shape[1]), lambda i: (i, 0)),
            pl.BlockSpec((1, size), lambda i: (0, i)),
            whole(size, size),
            whole(*qkv.shape),
            whole(*gate.shape),
            state_spec,
        ],
        out_specs=[whole(rows, value_dim), state_spec],
        scratch_shapes=[pltpu.VMEM((rows, value_dim), F32)],
        compiler_params=pltpu.CompilerParams(dimension_semantics=("arbitrary",)),
    )(decay, side, row, within, qkv, gate, state.reshape(batch_size, key_dim, value_dim))
    return h, new_state.reshape(state.shape)


class Ring:
    def __init__(self, n, rows, pieces):
        self.n, self.m = n, n // 2
        self.rows, self.pieces = rows, pieces
        self.size = rows // pieces
        me = lax.axis_index("tp")
        self.core = lax.rem(me, 2)
        chip = lax.div(me, 2)
        odd = lax.rem(chip, 2)
        half = lax.div(chip, 2)
        self.pos = (1 - odd) * half + odd * (self.m - 1 - half)
        self.me = me
        self.partner = chip * 2 + 1 - self.core
        self.right = self.device(self.pos + 1)
        self.left = self.device(self.pos - 1)

    def device(self, pos, other=False):
        m = self.m
        pos = lax.rem(pos + m, m)
        far = lax.div(pos, (m + 1) // 2)
        chip = (1 - far) * 2 * pos + far * (2 * (m - 1 - pos) + 1)
        return chip * 2 + (1 - self.core if other else self.core)

    def enter(self):
        barrier = pltpu.get_barrier_semaphore()
        for device in (self.left, self.right, self.partner):
            pl.semaphore_signal(barrier, inc=1, device_id={"tp": device}, device_id_type=MESH)
        pl.semaphore_wait(barrier, 3)

    def piece(self, j):
        return pl.ds(j * self.size, self.size)

    def clockwise(self, j):
        return j < self.pieces // 2

    def to(self, j):
        return self.right if self.clockwise(j) else self.left

    def back(self, j, steps):
        return self.pos - steps if self.clockwise(j) else self.pos + steps

    def order(self):
        half = self.pieces // 2
        return [j for pair in range(half) for j in (pair, pair + half)]


def remote(src, dst, send, recv, device):
    return pltpu.make_async_remote_copy(
        src_ref=src,
        dst_ref=dst,
        send_sem=send,
        recv_sem=recv,
        device_id={"tp": device},
        device_id_type=MESH,
    )


def gather_stage(ring, own_ref, whole, sems):
    width = own_ref.shape[1]
    send, recv, share_send, share_recv = sems

    def columns(device):
        return pl.ds(pl.multiple_of(device * width, width), width)

    whole[:, columns(ring.me)] = own_ref[...]
    hops, shares = {}, []
    for s in range(ring.m):
        for j in ring.order():
            rows = ring.piece(j)
            cols = columns(ring.device(ring.back(j, s)))
            if s > 0:
                hops[j, s - 1].wait_recv()
            src = own_ref.at[rows, :] if s == 0 else whole.at[rows, cols]
            if s < ring.m - 1:
                hop = remote(src, whole.at[rows, cols], send.at[j, s], recv.at[j, s], ring.to(j))
                hop.start()
                hops[j, s] = hop
            share = remote(
                src, whole.at[rows, cols], share_send.at[j, s], share_recv.at[j, s], ring.partner
            )
            share.start()
            shares.append(share)
    for hop in hops.values():
        hop.wait_send()
    for share in shares:
        share.wait()


def fill_weights(wq_ref, wk_ref, wv_ref, wg_ref, wcat):
    at = 0
    for ref in (wq_ref, wk_ref, wv_ref, wg_ref):
        wcat[:, at : at + ref.shape[1]] = ref[...]
        at += ref.shape[1]


def project_stage(whole, gain_ref, wcat, table_ref, qkv_ref, gate_ref, key_dim):
    rows, width = whole.shape
    tile = 16

    @pl.loop(0, rows // tile)
    def _(i):
        at = pl.ds(pl.multiple_of(i * tile, tile), tile)
        x = whole[at, :].astype(F32)
        inv = lax.rsqrt(jnp.mean(x * x, axis=-1, keepdims=True) + NORM_EPSILON)
        whole[at, :] = (x * inv * gain_ref[...]).astype(BF16)

    both = 2 * key_dim
    value_dim = gate_ref.shape[1]
    block = rows // 4

    @pl.loop(0, 4)
    def _(i):
        at = pl.ds(pl.multiple_of(i * block, block), block)
        out = jnp.dot(whole[at, :], wcat[...], preferred_element_type=F32)
        qk = out[:, :both]
        lane = lax.broadcasted_iota(jnp.int32, qk.shape, 1)
        ahead = pltpu.roll(qk, both - key_dim // 2, 1)
        behind = pltpu.roll(qk, key_dim // 2, 1)
        swapped = jnp.where(lax.rem(lane, key_dim) < key_dim // 2, ahead, behind)
        turned = qk * table_ref[at, :both] + swapped * table_ref[at, both:]
        qkv_ref[at, :both] = turned.astype(BF16)
        qkv_ref[at, both:] = out[:, both : both + value_dim].astype(BF16)
        gate = out[:, both + value_dim :]
        gate_ref[at, :] = gate / (1.0 + jnp.exp(-gate))


def scatter_stage(ring, h_ref, w_ref, x_ref, out_ref, h_pair, w_pair, outbox, inbox, sems):
    width = x_ref.shape[1]
    depth = h_ref.shape[1]
    send, recv, pair_send, pair_recv = sems
    w_copy = remote(
        w_ref, w_pair.at[pl.ds(depth, depth), :], pair_send.at[0], pair_recv.at[0], ring.partner
    )
    w_copy.start()
    h_copy = remote(
        h_ref, h_pair.at[:, pl.ds(depth, depth)], pair_send.at[1], pair_recv.at[1], ring.partner
    )
    h_copy.start()
    w_pair[:depth, :] = w_ref[...]
    h_pair[:, :depth] = h_ref[...]
    w_copy.wait()
    h_copy.wait()
    hops = {}
    for s in range(ring.m):
        for j in ring.order():
            rows = ring.piece(j)
            target = ring.device(ring.back(j, s + 1))
            cols = pl.ds(pl.multiple_of(target * width, width), width)
            part = jnp.dot(h_pair[rows, :], w_pair[:, cols], preferred_element_type=F32)
            if s > 0:
                hops[j, s - 1].wait_recv()
                part = part + inbox[j, s - 1].astype(F32)
            if s < ring.m - 1:
                outbox[j, s] = part.astype(BF16)
                hop = remote(
                    outbox.at[j, s], inbox.at[j, s], send.at[j, s], recv.at[j, s], ring.to(j)
                )
                hop.start()
                hops[j, s] = hop
            else:
                mix = part.astype(BF16).astype(F32)
                out_ref[rows, :] = (x_ref[rows, :].astype(F32) + mix).astype(BF16)
    for hop in hops.values():
        hop.wait_send()


def first_kernel(n, pieces, key_dim, *refs):
    x_ref, gain_ref, wq, wk, wv, wg, table, qkv, gate, whole, wcat, *sems = refs
    ring = Ring(n, x_ref.shape[0], pieces)
    ring.enter()
    fill_weights(wq, wk, wv, wg, wcat)
    gather_stage(ring, x_ref, whole, sems)
    project_stage(whole, gain_ref, wcat, table, qkv, gate, key_dim)


def middle_kernel(n, pieces, key_dim, *refs):
    h_ref, w_ref, x_ref, gain_ref, wq, wk, wv, wg, table = refs[:9]
    x1, qkv, gate, whole, wcat, h_pair, w_pair, outbox, inbox = refs[9:18]
    sems = refs[18:]
    ring = Ring(n, x_ref.shape[0], pieces)
    ring.enter()
    fill_weights(wq, wk, wv, wg, wcat)
    scatter_stage(ring, h_ref, w_ref, x_ref, x1, h_pair, w_pair, outbox, inbox, sems[4:])
    gather_stage(ring, x1, whole, sems[:4])
    project_stage(whole, gain_ref, wcat, table, qkv, gate, key_dim)


def last_kernel(n, pieces, *refs):
    h_ref, w_ref, x_ref, out_ref, h_pair, w_pair, outbox, inbox, *sems = refs
    ring = Ring(n, x_ref.shape[0], pieces)
    ring.enter()
    scatter_stage(ring, h_ref, w_ref, x_ref, out_ref, h_pair, w_pair, outbox, inbox, sems)


def gather_scratch(n, pieces, rows, width, wide):
    scratch = [pltpu.VMEM((rows, n * width), BF16), pltpu.VMEM((n * width, wide), BF16)]
    m = n // 2
    sems = [pltpu.SemaphoreType.DMA((pieces, m - 1))] * 2 + [pltpu.SemaphoreType.DMA((pieces, m))] * 2
    return scratch, sems


def scatter_scratch(n, pieces, rows, width, depth):
    m = n // 2
    boxes = pltpu.VMEM((pieces, m - 1, rows // pieces, width), BF16)
    scratch = [
        pltpu.VMEM((rows, 2 * depth), BF16),
        pltpu.VMEM((2 * depth, n * width), BF16),
        boxes,
        boxes,
    ]
    sems = [pltpu.SemaphoreType.DMA((pieces, m - 1))] * 2 + [pltpu.SemaphoreType.DMA((2,))] * 2
    return scratch, sems


def call(kernel, outs, scratch, collective_id, *args):
    vmem = pl.BlockSpec(memory_space=pltpu.VMEM)
    return pl.pallas_call(
        kernel,
        out_shape=outs,
        in_specs=[vmem] * len(args),
        out_specs=[vmem] * len(outs),
        scratch_shapes=scratch,
        compiler_params=pltpu.CompilerParams(
            collective_id=collective_id, has_side_effects=True, vmem_limit_bytes=56 * 2**20
        ),
    )(*args)


def plain_project(x, gain, weights, table, key_dim):
    whole = lax.all_gather(x, "tp", axis=1, tiled=True).astype(F32)
    inv = lax.rsqrt(jnp.mean(whole * whole, axis=-1, keepdims=True) + NORM_EPSILON)
    normed = (whole * inv * gain).astype(BF16)
    qk = jnp.dot(normed, jnp.concatenate(weights[:2], axis=1), preferred_element_type=F32)
    halves = qk.reshape(qk.shape[0], 2, 2, key_dim // 2)
    swapped = halves[:, :, ::-1].reshape(qk.shape)
    turned = qk * table[:, : 2 * key_dim] + swapped * table[:, 2 * key_dim :]
    values = jnp.dot(normed, weights[2], preferred_element_type=F32)
    gate = jnp.dot(normed, weights[3], preferred_element_type=F32)
    qkv = jnp.concatenate([turned.astype(BF16), values.astype(BF16)], axis=1)
    return qkv, jax.nn.silu(gate)


def plain_finish(h, w_out, x):
    part = jnp.dot(h, w_out, preferred_element_type=F32).astype(BF16)
    mix = lax.psum_scatter(part, "tp", scatter_dimension=1, tiled=True)
    return (x.astype(F32) + mix.astype(F32)).astype(BF16)


def shards(
    tokens,
    lengths,
    gain_first,
    query_first,
    key_first,
    value_first,
    gate_first,
    out_first,
    state_first,
    gain_second,
    query_second,
    key_second,
    value_second,
    gate_second,
    out_second,
    state_second,
):
    n = lax.axis_size("tp")
    batch_size, head_count, key_dim, value_dim = state_first.shape
    slots, width = tokens.shape
    block_len = slots // batch_size
    rows = LIVE_TOTAL

    lengths_i = lengths.astype(jnp.int32)
    starts = jnp.cumsum(lengths_i) - lengths_i
    slot = jnp.arange(block_len, dtype=jnp.int32)
    live = slot[None, :] < lengths_i[:, None]
    target = jnp.where(live, starts[:, None] + slot[None, :], -1).reshape(slots)
    pack = (jnp.arange(rows, dtype=jnp.int32)[:, None] == target[None, :]).astype(BF16)

    def packed(padded):
        return jnp.dot(pack, padded, preferred_element_type=F32)

    def spread(rows_in):
        return lax.dot_general(
            pack, rows_in, (((0,), (0,)), ((), ())), preferred_element_type=F32
        ).astype(rows_in.dtype)

    slot_hot = jnp.tile(jnp.eye(block_len, dtype=BF16), (batch_size, 1))
    table = jnp.dot(
        packed(slot_hot), rope_tables(block_len, key_dim), precision=lax.Precision.HIGHEST
    )
    x = packed(tokens).astype(BF16)

    weights_first = (query_first, key_first, value_first, gate_first)
    weights_second = (query_second, key_second, value_second, gate_second)
    wide = sum(w.shape[1] for w in weights_first)
    pieces = next((p for p in (6, 4, 2) if rows % (16 * p) == 0), 0)
    ringed = (
        n >= 4
        and n % 2 == 0
        and pieces > 0
        and rows % 64 == 0
        and head_count == 1
        and width % 128 == 0
        and value_dim % 128 == 0
        and 2 * key_dim % 128 == 0
    )
    size = 128
    grouped = (
        head_count == 1
        and size % (2 * block_len) == 0
        and slots % size == 0
        and 2 * key_dim == 128
        and value_dim % 128 == 0
        and rows % 16 == 0
    )
    if grouped:
        log_gamma = decay_logs(1)[0]
        slot_f, count = slot.astype(F32), lengths_i.astype(F32)
        inward = jnp.broadcast_to(jnp.exp(log_gamma * (slot_f + 1.0))[None, :], live.shape)
        gap = jnp.maximum(count[:, None] - 1.0 - slot_f[None, :], 0.0)
        onward = jnp.exp(log_gamma * gap)
        side = jnp.stack([target.astype(F32), inward.reshape(slots), onward.reshape(slots)], axis=1)
        decay = jnp.exp(log_gamma * count)
        r = jnp.arange(size, dtype=jnp.int32)
        step = (r[:, None] - r[None, :]).astype(F32)
        same = (r[:, None] // block_len == r[None, :] // block_len) & (step >= 0.0)
        within = jnp.where(same, jnp.exp(log_gamma * jnp.maximum(step, 0.0)), 0.0)

    def retention(qkv, gate, state):
        if grouped:
            return retain_packed(
                decay, side, target[None, :], within, qkv, gate, state, block_len
            )
        normed, new_state = retain(spread(qkv), lengths, state)
        return (packed(normed) * gate).astype(BF16), new_state

    outs = [
        jax.ShapeDtypeStruct((rows, 2 * key_dim + value_dim), BF16),
        jax.ShapeDtypeStruct((rows, value_dim), F32),
    ]
    own = jax.ShapeDtypeStruct((rows, width), BF16)
    gather_bufs, gather_sems = gather_scratch(n, pieces or 2, rows, width, wide)
    scatter_bufs, scatter_sems = scatter_scratch(n, pieces or 2, rows, width, value_dim)

    if ringed:
        qkv, gate = call(
            functools.partial(first_kernel, n, pieces, key_dim),
            outs,
            gather_bufs + gather_sems,
            0,
            x,
            gain_first[None],
            *weights_first,
            table,
        )
    else:
        qkv, gate = plain_project(x, gain_first, weights_first, table, key_dim)
    h, state_first_new = retention(qkv, gate, state_first)
    if ringed:
        x1, qkv, gate = call(
            functools.partial(middle_kernel, n, pieces, key_dim),
            [own] + outs,
            gather_bufs + scatter_bufs + gather_sems + scatter_sems,
            1,
            h,
            out_first,
            x,
            gain_second[None],
            *weights_second,
            table,
        )
    else:
        x1 = plain_finish(h, out_first, x)
        qkv, gate = plain_project(x1, gain_second, weights_second, table, key_dim)
    h, state_second_new = retention(qkv, gate, state_second)
    if ringed:
        (y,) = call(
            functools.partial(last_kernel, n, pieces),
            [own],
            scatter_bufs + scatter_sems,
            2,
            h,
            out_second,
            x1,
        )
    else:
        y = plain_finish(h, out_second, x1)
    mixed_out = jnp.where(live.reshape(slots, 1), spread(y), tokens)
    return (mixed_out, state_first_new, state_second_new)


def solution(mesh):
    heads = P(None, "tp")
    state = P("grp", "tp", None, None)
    block = (P(), heads, heads, heads, heads, P("tp", None), state)
    in_specs = (P("grp", "tp"), P("grp")) + block + block
    out_specs = (P("grp", "tp"), state, state)
    return jax.shard_map(shards, mesh=mesh, in_specs=in_specs, out_specs=out_specs, check_vma=False)
```

profile of v0, /device:TPU:0, one launch (start us, length us, event | category | flops | bytes accessed | tf_op | source)
XLA Modules:
  0.0 208.7 jit_solution(13558564685641056511)
XLA Ops:
  0.8 1.2 convert_add_fusion
  2.0 0.1 multiply_exponential_fusion
  2.1 0.7 iota_compare_fusion.10
  2.8 0.1 lt.42
  2.9 0.1 multiply_sine_fusion
  3.1 0.1 maximum_multiply_fusion
  3.1 0.1 concatenate.12
  3.2 0.1 copy.46
  3.3 0.1 exp.29
  3.4 0.1 stack_reshape.4
  3.5 0.8 copy.45
  4.3 0.1 reduce-window.9
  4.4 0.1 reduce
  4.5 0.7 sub.64
  5.2 0.7 exponential_select_fusion.refs_3_
  5.9 0.7 broadcast_select_fusion
  6.6 0.7 select_n.54.refs_2_
  7.3 0.1 convert_element_type.54
  7.4 0.1 add.77
  7.5 0.0 copy-start
  7.5 2.8 %fusion.8.refs_0_.refs_2_ = bf16[960,128]{1,0:T(8,128)(2,1)} fusion(bf16[1536,128]{1,0:T(8,128)(2,1)} %param.16, s32[1536]{0:T(1024)S(1)} %broadcast_select_fusion.1), kind=kOutput, calls=%fused_computation.9 | convolution fusion | flops 379084800 | bytes 645120 | tf_op jit(solution)/shard_map/dot_general | solution.py:465
  10.3 0.0 copy-start.1
  10.3 0.0 copy-start.2
  10.3 0.0 copy-start.3
  10.3 0.1 tile.4
  10.4 1.1 fusion.1
  11.5 0.0 copy-done
  11.5 1.0 copy.47.refs_2_
  12.5 0.0 copy-done.1
  12.5 1.0 copy.48.refs_3_
  13.6 0.0 copy-done.2
  13.6 1.0 copy.50.refs_4_
  14.6 0.0 copy-done.3
  14.6 1.0 copy.51.refs_5_
  15.6 1.2 copy.52.refs_1_
  16.8 1.9 fusion.13.refs_6_.refs_8_
  18.7 44.8 %shard_map.175 = (bf16[960,256]{1,0:T(8,128)(2,1)}, f32[960,128]{1,0:T(8,128)}) custom-call(bf16[960,128]{1,0:T(8,128)(2,1)} %fusion.8.refs_0_.refs_2_, f32[1,2048]{1,0:T(1,128)} %bitcast.20, bf16[2048,64]{1,0:T(8,128)(2,1)} %copy.47.refs_2_, bf16[2048,64]{1,0:T(8,128)(2,1)} %copy.48.refs_3_, bf16[2048,128]{1,0:T(8,128)(2,1)} %refs_4_.2, ...), custom_call_target="tpu_custom_call" | custom-call | tf_op jit(solution)/shard_map/pallas_call | solution.py:401
  63.5 19.9 %shard_map.176 = (bf16[960,128]{1,0:T(8,128)(2,1)}, f32[96,64,128]{2,1,0:T(8,128)}) custom-call(f32[96]{0:T(128)} %get-tuple-element.40.refs_0_, f32[1536,3]{1,0:T(8,128)} %copy.52.refs_1_, s32[1,1536]{1,0:T(1,128)} %select_n.54.refs_2_, f32[128,128]{1,0:T(8,128)} %exponential_select_fusion.refs_3_, bf16[960,256]{1,0:T(8,128)(2,1)} %get-tuple-element.12.refs_4_, ...), custom_call_target="tpu_custom_call" | custom-call | tf_op jit(solution)/shard_map/pallas_call | solution.py:162
  83.4 70.3 %shard_map.177 = (bf16[960,128]{1,0:T(8,128)(2,1)}, bf16[960,256]{1,0:T(8,128)(2,1)}, f32[960,128]{1,0:T(8,128)}) custom-call(bf16[960,128]{1,0:T(8,128)(2,1)} %get-tuple-element.14.refs_0_, bf16[128,2048]{1,0:T(8,128)(2,1)} %refs_1_.2, bf16[960,128]{1,0:T(8,128)(2,1)} %fusion.8.refs_0_.refs_2_, f32[1,2048]{1,0:T(1,128)} %bitcast.21, ...), custom_call_target="tpu_custom_call" | custom-call | tf_op jit(solution)/shard_map/pallas_call | solution.py:401
  153.7 0.0 copy-start.4
  153.7 20.0 %shard_map.178 = (bf16[960,128]{1,0:T(8,128)(2,1)}, f32[96,64,128]{2,1,0:T(8,128)}) custom-call(f32[96]{0:T(128)} %get-tuple-element.40.refs_0_, f32[1536,3]{1,0:T(8,128)} %copy.52.refs_1_, s32[1,1536]{1,0:T(1,128)} %select_n.54.refs_2_, f32[128,128]{1,0:T(8,128)} %exponential_select_fusion.refs_3_, bf16[960,256]{1,0:T(8,128)(2,1)} %get-tuple-element.15.refs_4_, ...), custom_call_target="tpu_custom_call" | custom-call | tf_op jit(solution)/shard_map/pallas_call | solution.py:162
  173.7 31.4 %shard_map.179 = bf16[960,128]{1,0:T(8,128)(2,1)} custom-call(bf16[960,128]{1,0:T(8,128)(2,1)} %get-tuple-element.17.refs_0_, bf16[128,2048]{1,0:T(8,128)(2,1)} %refs_1_.3, bf16[960,128]{1,0:T(8,128)(2,1)} %get-tuple-element.18.refs_2_), custom_call_target="tpu_custom_call" | custom-call | tf_op jit(solution)/shard_map/pallas_call | solution.py:401
  205.1 0.0 copy-done.4
  205.1 3.6 %fusion.7 = bf16[1536,128]{1,0:T(8,128)(2,1)} fusion(bf16[1536,128]{1,0:T(8,128)(2,1)S(1)} %copy-done.4, bf16[960,128]{1,0:T(8,128)(2,1)} %shard_map.179, s32[1536]{0:T(1024)S(1)} %broadcast_select_fusion.1, pred[1536]{0:T(1024)(128)(4,1)S(1)} %lt.42), kind=kOutput, calls=%fused_computation.8 | convolution fusion | flops 379355136 | bytes 1039872 | tf_op jit(solution)/shard_map/dot_general | solution.py:468
  (9 shorter events, 0.1 us)
Async XLA Ops:
  7.5 4.0 %copy-start = (bf16[2048,64]{0,1:T(8,128)(2,1)S(1)}, bf16[2048,64]{0,1:T(8,128)(2,1)}, u32[]{:S(2)}) copy-start(bf16[2048,64]{0,1:T(8,128)(2,1)} %param.19) | copy-start | bytes 786436
  10.3 2.2 %copy-start.1 = (bf16[2048,64]{0,1:T(8,128)(2,1)S(1)}, bf16[2048,64]{0,1:T(8,128)(2,1)}, u32[]{:S(2)}) copy-start(bf16[2048,64]{0,1:T(8,128)(2,1)} %param.20) | copy-start | bytes 786436
  10.3 3.2 %copy-start.2 = (bf16[2048,64]{0,1:T(8,128)(2,1)S(1)}, bf16[2048,64]{0,1:T(8,128)(2,1)}, u32[]{:S(2)}) copy-start(bf16[2048,64]{0,1:T(8,128)(2,1)} %param.26) | copy-start | bytes 786436
  10.3 4.2 %copy-start.3 = (bf16[2048,64]{0,1:T(8,128)(2,1)S(1)}, bf16[2048,64]{0,1:T(8,128)(2,1)}, u32[]{:S(2)}) copy-start(bf16[2048,64]{0,1:T(8,128)(2,1)} %param.27) | copy-start | bytes 786436
  153.7 51.4 %copy-start.4 = (bf16[1536,128]{1,0:T(8,128)(2,1)S(1)}, bf16[1536,128]{1,0:T(8,128)(2,1)}, u32[]{:S(2)}) copy-start(bf16[1536,128]{1,0:T(8,128)(2,1)} %param.16) | copy-start | bytes 1179652
where the time goes:
time: 209 us
  Pallas kernels  186 us (89%)
  matrix products  9.46 us (5%)
  local copies, waits for them, and re-layouts  7.36 us (4%)
  other arithmetic  4.66 us (2%)
    pallas_call x3, Pallas kernels, call(): pl.pallas_call(kernel, out_shape=outs, in_specs=[vmem] * len(args), out_s...  146 us
    pallas_call x2, Pallas kernels, retain_packed(): pl.pallas_call(functools.partial(retention_kernel, key_dim, block_len), g...  39.9 us

commit v1 on v0

--- a/solution.py
+++ b/solution.py
@@ -85,43 +85,62 @@
     rows = qkv_ref.shape[0]
     both = 2 * key_dim
     size = side_ref.shape[0]
-    group = size // block_len
     side = side_ref[...]
+    unit = within_ref.shape[0]
+    group = unit // block_len
 
     slots = lax.broadcasted_iota(jnp.int32, (size, rows), 1)
     hot = jnp.where(slots == side[:, 0:1].astype(jnp.int32), 1.0, 0.0).astype(BF16)
     padded = jnp.dot(hot, qkv_ref[...], preferred_element_type=F32)
-    qk, values = padded[:, :both], padded[:, both:].astype(BF16)
-    front = lax.broadcasted_iota(jnp.int32, qk.shape, 1) < key_dim
-    turned = pltpu.roll(qk, key_dim, 1)
-    queries, keys = jnp.where(front, qk, turned), jnp.where(front, turned, qk)
-    scores = lax.dot_general(
-        jnp.where(front, qk, 0.0).astype(BF16),
-        keys.astype(BF16),
-        (((1,), (1,)), ((), ())),
-        preferred_element_type=F32,
-    )
-    weights = (scores * within_ref[...]).astype(BF16)
-    retained = jnp.dot(weights, values, preferred_element_type=F32)
-
-    wide = (size, group * key_dim)
+    wide = (unit, group * key_dim)
     own = lax.div(lax.broadcasted_iota(jnp.int32, wide, 0), block_len) == lax.div(
         lax.broadcasted_iota(jnp.int32, wide, 1), key_dim
     )
+    front = lax.broadcasted_iota(jnp.int32, (unit, both), 1) < key_dim
 
     def per_sequence(doubled):
         spread = jnp.concatenate([doubled] * (group // 2), axis=1)
         return jnp.where(own, spread, 0.0).astype(BF16)
 
-    state = state_ref[...].reshape(group * key_dim, state_ref.shape[-1])
-    high = state.astype(BF16)
-    low = (state - high.astype(F32)).astype(BF16)
-    wide_q = per_sequence(queries)
-    carried = jnp.dot(wide_q, high, preferred_element_type=F32)
-    carried = carried + jnp.dot(wide_q, low, preferred_element_type=F32)
-    retained = retained + carried * side[:, 1:2]
-    inv = lax.rsqrt(jnp.mean(retained * retained, axis=-1, keepdims=True) + NORM_EPSILON)
-    normed = (retained * inv).astype(BF16)
+    def one(u):
+        at = slice(u * unit, (u + 1) * unit)
+        first = u * group
+        qk, values = padded[at, :both], padded[at, both:].astype(BF16)
+        turned = pltpu.roll(qk, key_dim, 1)
+        queries, keys = jnp.where(front, qk, turned), jnp.where(front, turned, qk)
+        scores = lax.dot_general(
+            jnp.where(front, qk, 0.0).astype(BF16),
+            keys.astype(BF16),
+            (((1,), (1,)), ((), ())),
+            preferred_element_type=F32,
+        )
+        weights = (scores * within_ref[...]).astype(BF16)
+        retained = jnp.dot(weights, values, preferred_element_type=F32)
+        state = state_ref[first : first + group].reshape(group * key_dim, state_ref.shape[-1])
+        high = state.astype(BF16)
+        low = (state - high.astype(F32)).astype(BF16)
+        wide_q = per_sequence(queries)
+        carried = jnp.dot(wide_q, high, preferred_element_type=F32)
+        carried = carried + jnp.dot(wide_q, low, preferred_element_type=F32)
+        retained = retained + carried * side[at, 1:2]
+        inv = lax.rsqrt(jnp.mean(retained * retained, axis=-1, keepdims=True) + NORM_EPSILON)
+
+        scaled = keys * side[at, 2:3]
+        k_high = scaled.astype(BF16).astype(F32)
+        added = None
+        for piece in (k_high, scaled - k_high):
+            term = lax.dot_general(
+                per_sequence(piece), values, (((0,), (0,)), ((), ())), preferred_element_type=F32
+            )
+            added = term if added is None else added + term
+        for b in range(group):
+            new_ref[first + b] = (
+                state_ref[first + b] * decay[i * (size // block_len) + first + b]
+                + added[b * key_dim : (b + 1) * key_dim, :]
+            )
+        return (retained * inv).astype(BF16)
+
+    normed = jnp.concatenate([one(u) for u in range(size // unit)], axis=0)
     places = lax.broadcasted_iota(jnp.int32, (rows, size), 0)
     back = jnp.where(places == row_ref[...], 1.0, 0.0).astype(BF16)
     part = jnp.dot(back, normed, preferred_element_type=F32)
@@ -134,19 +153,6 @@
     def _():
         total[...] += part
 
-    scaled = keys * side[:, 2:3]
-    k_high = scaled.astype(BF16).astype(F32)
-    added = None
-    for piece in (k_high, scaled - k_high):
-        term = lax.dot_general(
-            per_sequence(piece), values, (((0,), (0,)), ((), ())), preferred_element_type=F32
-        )
-        added = term if added is None else added + term
-    for b in range(group):
-        new_ref[b] = (
-            state_ref[b] * decay[i * group + b] + added[b * key_dim : (b + 1) * key_dim, :]
-        )
-
     @pl.when(i == pl.num_programs(0) - 1)
     def _():
         h_ref[...] = (total[...] * gate_ref[...]).astype(BF16)
@@ -155,7 +161,9 @@
 def retain_packed(decay, side, row, within, qkv, gate, state, block_len):
     batch_size, _, key_dim, value_dim = state.shape
     rows = qkv.shape[0]
-    size = within.shape[0]
+    unit = within.shape[0]
+    many = next(k for k in (3, 2, 1) if batch_size * block_len % (k * unit) == 0)
+    size = many * unit
     group = size // block_len
     whole = lambda *shape: pl.BlockSpec(shape, lambda i: (0,) * len(shape))
     state_spec = pl.BlockSpec((group, key_dim, value_dim), lambda i: (i, 0, 0))
@@ -170,7 +178,7 @@
             pl.BlockSpec(memory_space=pltpu.SMEM),
             pl.BlockSpec((size, side.shape[1]), lambda i: (i, 0)),
             pl.BlockSpec((1, size), lambda i: (0, i)),
-            whole(size, size),
+            whole(unit, unit),
             whole(*qkv.shape),
             whole(*gate.shape),
             state_spec,
@@ -239,15 +247,22 @@
     )
 
 
-def gather_stage(ring, own_ref, whole, sems):
+def gather_stage(ring, own_ref, whole, sems, prepare, consume):
     width = own_ref.shape[1]
     send, recv, share_send, share_recv = sems
 
     def columns(device):
         return pl.ds(pl.multiple_of(device * width, width), width)
 
-    whole[:, columns(ring.me)] = own_ref[...]
-    hops, shares = {}, []
+    hops, shares = {}, {}
+
+    def use(s):
+        for j in range(ring.pieces):
+            shares[j, s].wait_recv()
+        for way in (0, ring.pieces // 2):
+            chip = lax.div(ring.device(ring.back(way, s)), 2)
+            consume(way * ring.size, chip)
+
     for s in range(ring.m):
         for j in ring.order():
             rows = ring.piece(j)
@@ -263,31 +278,62 @@
                 src, whole.at[rows, cols], share_send.at[j, s], share_recv.at[j, s], ring.partner
             )
             share.start()
-            shares.append(share)
+            shares[j, s] = share
+        if s == 0:
+            whole[:, columns(ring.me)] = own_ref[...]
+            prepare()
+        else:
+            use(s - 1)
+    use(ring.m - 1)
     for hop in hops.values():
         hop.wait_send()
-    for share in shares:
-        share.wait()
-
-
-def fill_weights(wq_ref, wk_ref, wv_ref, wg_ref, wcat):
-    at = 0
-    for ref in (wq_ref, wk_ref, wv_ref, wg_ref):
-        wcat[:, at : at + ref.shape[1]] = ref[...]
-        at += ref.shape[1]
-
-
-def project_stage(whole, gain_ref, wcat, table_ref, qkv_ref, gate_ref, key_dim):
-    rows, width = whole.shape
-    tile = 16
-
-    @pl.loop(0, rows // tile)
+    for share in shares.values():
+        share.wait_send()
+
+
+def fill_weights(wq_ref, wk_ref, wv_ref, wg_ref, wcat, total, squares):
+    both = 2 * wq_ref.shape[0]
+    step = 128
+
+    @pl.loop(0, wcat.shape[0] // step)
     def _(i):
-        at = pl.ds(pl.multiple_of(i * tile, tile), tile)
-        x = whole[at, :].astype(F32)
-        inv = lax.rsqrt(jnp.mean(x * x, axis=-1, keepdims=True) + NORM_EPSILON)
-        whole[at, :] = (x * inv * gain_ref[...]).astype(BF16)
-
+        at = pl.ds(pl.multiple_of(i * step, step), step)
+        pair = jnp.concatenate([wq_ref[:, at], wk_ref[:, at]], axis=0)
+        wcat[at, :both] = jnp.transpose(pair.astype(F32)).astype(BF16)
+
+    mid = both + wv_ref.shape[1]
+    wcat[:, both:mid] = wv_ref[...]
+    wcat[:, mid:] = wg_ref[...]
+    total[...] = jnp.zeros_like(total)
+    squares[...] = jnp.zeros_like(squares)
+
+
+def consumer(whole, width, gain_ref, wcat, total, squares):
+    half = whole.shape[0] // 2
+    block = half // 2
+
+    def consume(first, chip):
+        cols = pl.ds(pl.multiple_of(chip * 2 * width, 2 * width), 2 * width)
+        gain = gain_ref[:, cols]
+
+        @pl.loop(0, 2)
+        def _(i):
+            at = pl.ds(pl.multiple_of(first + i * block, 16), block)
+            x = whole[at, cols].astype(F32)
+            square = x * x
+            part = square[:, :128]
+            for k in range(128, 2 * width, 128):
+                part = part + square[:, k : k + 128]
+            squares[at, :] += part
+            total[at, :] += jnp.dot(
+                (x * gain).astype(BF16), wcat[cols, :], preferred_element_type=F32
+            )
+
+    return consume
+
+
+def project_stage(width, total, squares, table_ref, qkv_ref, gate_ref, key_dim):
+    rows = total.shape[0]
     both = 2 * key_dim
     value_dim = gate_ref.shape[1]
     block = rows // 4
@@ -295,7 +341,8 @@
     @pl.loop(0, 4)
     def _(i):
         at = pl.ds(pl.multiple_of(i * block, block), block)
-        out = jnp.dot(whole[at, :], wcat[...], preferred_element_type=F32)
+        mean = jnp.sum(squares[at, :], axis=-1, keepdims=True) / width
+        out = total[at, :] * lax.rsqrt(mean + NORM_EPSILON)
         qk = out[:, :both]
         lane = lax.broadcasted_iota(jnp.int32, qk.shape, 1)
         ahead = pltpu.roll(qk, both - key_dim // 2, 1)
@@ -308,7 +355,7 @@
         gate_ref[at, :] = gate / (1.0 + jnp.exp(-gate))
 
 
-def scatter_stage(ring, h_ref, w_ref, x_ref, out_ref, h_pair, w_pair, outbox, inbox, sems):
+def scatter_stage(ring, h_ref, w_ref, x_ref, out_ref, h_pair, w_pair, outbox, inbox, sems, prepare):
     width = x_ref.shape[1]
     depth = h_ref.shape[1]
     send, recv, pair_send, pair_recv = sems
@@ -320,6 +367,7 @@
         h_ref, h_pair.at[:, pl.ds(depth, depth)], pair_send.at[1], pair_recv.at[1], ring.partner
     )
     h_copy.start()
+    prepare()
     w_pair[:depth, :] = w_ref[...]
     h_pair[:, :depth] = h_ref[...]
     w_copy.wait()
@@ -348,36 +396,51 @@
         hop.wait_send()
 
 
+def nothing():
+    pass
+
+
 def first_kernel(n, pieces, key_dim, *refs):
-    x_ref, gain_ref, wq, wk, wv, wg, table, qkv, gate, whole, wcat, *sems = refs
+    x_ref, gain_ref, wq, wk, wv, wg, table, qkv, gate, whole, wcat, total, squares, *sems = refs
     ring = Ring(n, x_ref.shape[0], pieces)
     ring.enter()
-    fill_weights(wq, wk, wv, wg, wcat)
-    gather_stage(ring, x_ref, whole, sems)
-    project_stage(whole, gain_ref, wcat, table, qkv, gate, key_dim)
+    fill = functools.partial(fill_weights, wq, wk, wv, wg, wcat, total, squares)
+    consume = consumer(whole, x_ref.shape[1], gain_ref, wcat, total, squares)
+    gather_stage(ring, x_ref, whole, sems, fill, consume)
+    project_stage(whole.shape[1], total, squares, table, qkv, gate, key_dim)
 
 
 def middle_kernel(n, pieces, key_dim, *refs):
     h_ref, w_ref, x_ref, gain_ref, wq, wk, wv, wg, table = refs[:9]
-    x1, qkv, gate, whole, wcat, h_pair, w_pair, outbox, inbox = refs[9:18]
-    sems = refs[18:]
+    x1, qkv, gate, whole, wcat, total, squares, h_pair, w_pair, outbox, inbox = refs[9:20]
+    sems = refs[20:]
     ring = Ring(n, x_ref.shape[0], pieces)
     ring.enter()
-    fill_weights(wq, wk, wv, wg, wcat)
-    scatter_stage(ring, h_ref, w_ref, x_ref, x1, h_pair, w_pair, outbox, inbox, sems[4:])
-    gather_stage(ring, x1, whole, sems[:4])
-    project_stage(whole, gain_ref, wcat, table, qkv, gate, key_dim)
+    fill = functools.partial(fill_weights, wq, wk, wv, wg, wcat, total, squares)
+    consume = consumer(whole, x_ref.shape[1], gain_ref, wcat, total, squares)
+    scatter_stage(
+        ring, h_ref, w_ref, x_ref, x1, h_pair, w_pair, outbox, inbox, sems[4:], fill
+    )
+    gather_stage(ring, x1, whole, sems[:4], nothing, consume)
+    project_stage(whole.shape[1], total, squares, table, qkv, gate, key_dim)
 
 
 def last_kernel(n, pieces, *refs):
     h_ref, w_ref, x_ref, out_ref, h_pair, w_pair, outbox, inbox, *sems = refs
     ring = Ring(n, x_ref.shape[0], pieces)
     ring.enter()
-    scatter_stage(ring, h_ref, w_ref, x_ref, out_ref, h_pair, w_pair, outbox, inbox, sems)
+    scatter_stage(
+        ring, h_ref, w_ref, x_ref, out_ref, h_pair, w_pair, outbox, inbox, sems, nothing
+    )
 
 
 def gather_scratch(n, pieces, rows, width, wide):
-    scratch = [pltpu.VMEM((rows, n * width), BF16), pltpu.VMEM((n * width, wide), BF16)]
+    scratch = [
+        pltpu.VMEM((rows, n * width), BF16),
+        pltpu.VMEM((n * width, wide), BF16),
+        pltpu.VMEM((rows, wide), F32),
+        pltpu.VMEM((rows, 128), F32),
+    ]
     m = n // 2
     sems = [pltpu.SemaphoreType.DMA((pieces, m - 1))] * 2 + [pltpu.SemaphoreType.DMA((pieces, m))] * 2
     return scratch, sems
@@ -478,7 +541,7 @@
     weights_first = (query_first, key_first, value_first, gate_first)
     weights_second = (query_second, key_second, value_second, gate_second)
     wide = sum(w.shape[1] for w in weights_first)
-    pieces = next((p for p in (6, 4, 2) if rows % (16 * p) == 0), 0)
+    pieces = next((p for p in (10, 6, 4, 2) if rows % (16 * p) == 0), 0)
     ringed = (
         n >= 4
         and n % 2 == 0
@@ -527,6 +590,9 @@
     gather_bufs, gather_sems = gather_scratch(n, pieces or 2, rows, width, wide)
     scatter_bufs, scatter_sems = scatter_scratch(n, pieces or 2, rows, width, value_dim)
 
+    def turned(weights):
+        return (weights[0].T, weights[1].T) + weights[2:]
+
     if ringed:
         qkv, gate = call(
             functools.partial(first_kernel, n, pieces, key_dim),
@@ -535,7 +601,7 @@
             0,
             x,
             gain_first[None],
-            *weights_first,
+            *turned(weights_first),
             table,
         )
     else:
@@ -551,7 +617,7 @@
             out_first,
             x,
             gain_second[None],
-            *weights_second,
+            *turned(weights_second),
             table,
         )
     else:

time: 209 us -> 166 us (0.79)
  Pallas kernels: 186 us -> 148 us
  local copies, waits for them, and re-layouts: 7.36 us -> 3.32 us
    pallas_call x2, Pallas kernels: 39.9 us -> 19.9 us  [retain_packed(): pl.pallas_call(functools.partial(retention_kernel, key_dim, block_len), g...]
    pallas_call x3, Pallas kernels: 146 us -> 128 us  [call(): pl.pallas_call(kernel, out_shape=outs, in_specs=[vmem] * len(args), out_s...]
    unnamed x14 -> x2, local copies, waits for them, and re-layouts: 4.07 us -> 0.01 us
where the time goes in v1:
time: 166 us
  Pallas kernels  148 us (89%)
  matrix products  9.43 us (6%)
  other arithmetic  4.61 us (3%)
  local copies, waits for them, and re-layouts  3.32 us (2%)
    pallas_call x3, Pallas kernels, call(): pl.pallas_call(kernel, out_shape=outs, in_specs=[vmem] * len(args), out_s...  128 us
    pallas_call x2, Pallas kernels, retain_packed(): pl.pallas_call(functools.partial(retention_kernel, key_dim, block_len), g...  19.9 us
    dot_general x2, matrix products, packed(): return jnp.dot(pack, padded, preferred_element_type=F32)  3.88 us
    dot_general x1, matrix products, spread(): lax.dot_general(pack, rows_in, (((0,), (0,)), ((), ())), preferred_elemen...  3.63 us

profile of v1, /device:TPU:0, one launch (start us, length us, event | category | flops | bytes accessed | tf_op | source)
XLA Modules:
  0.0 165.8 jit_solution(1174681591281710253)
XLA Ops:
  0.8 1.2 convert_add_fusion
  2.0 0.1 multiply_exponential_fusion
  2.0 0.7 iota_compare_fusion.10
  2.8 0.1 lt.42
  2.9 0.1 multiply_sine_fusion
  3.0 0.1 maximum_multiply_fusion
  3.1 0.1 concatenate.12
  3.2 0.1 copy.34
  3.3 0.1 exp.29
  3.4 0.1 stack_reshape.4
  3.5 0.8 copy.33
  4.2 0.1 reduce-window.9
  4.3 0.1 reduce
  4.5 0.7 sub.64
  5.1 0.7 exponential_select_fusion.refs_3_
  5.8 0.7 broadcast_select_fusion
  6.6 0.7 select_n.54.refs_2_
  7.3 0.1 convert_element_type.54
  7.4 0.1 add.77
  7.5 2.7 %fusion.8.refs_0_.refs_2_ = bf16[960,128]{1,0:T(8,128)(2,1)} fusion(bf16[1536,128]{1,0:T(8,128)(2,1)} %param.16, s32[1536]{0:T(1024)S(1)} %broadcast_select_fusion.1), kind=kOutput, calls=%fused_computation.9 | convolution fusion | flops 379084800 | bytes 645120 | tf_op jit(solution)/shard_map/dot_general | solution.py:528
  10.2 0.1 tile.4
  10.3 1.1 fusion.1
  11.4 1.2 copy.36.refs_1_
  12.6 1.9 %fusion.13.refs_6_.refs_8_ = f32[960,256]{1,0:T(8,128)} fusion(f32[960,16]{0,1:T(8,128)S(1)} %fusion.1, f32[16,256]{1,0:T(8,128)S(1)} %concatenate.12), kind=kOutput, calls=%fused_computation.38 | convolution fusion | flops 47185920 | bytes 1060864 | tf_op jit(solution)/shard_map/dot_general | solution.py:536
  14.5 35.9 %shard_map.175 = (bf16[960,256]{1,0:T(8,128)(2,1)}, f32[960,128]{1,0:T(8,128)}) custom-call(bf16[960,128]{1,0:T(8,128)(2,1)} %fusion.8.refs_0_.refs_2_, f32[1,2048]{1,0:T(1,128)} %bitcast.28, bf16[64,2048]{1,0:T(8,128)(2,1)} %bitcast.26, bf16[64,2048]{1,0:T(8,128)(2,1)} %bitcast.27, bf16[2048,128]{1,0:T(8,128)(2,1)} %refs_4_.1, bf16[2048,128]{1,0:T(8,128)(2,1)} %refs_5_.1, ...), custom_call_target="tpu_custom_call" | custom-call | tf_op jit(solution)/shard_map/pallas_call | solution.py:464
  50.5 10.0 %shard_map.176 = (bf16[960,128]{1,0:T(8,128)(2,1)}, f32[96,64,128]{2,1,0:T(8,128)}) custom-call(f32[96]{0:T(128)} %get-tuple-element.40.refs_0_, f32[1536,3]{1,0:T(8,128)} %copy.36.refs_1_, s32[1,1536]{1,0:T(1,128)} %select_n.54.refs_2_, f32[128,128]{1,0:T(8,128)} %exponential_select_fusion.refs_3_, bf16[960,256]{1,0:T(8,128)(2,1)} %get-tuple-element.12.refs_4_, ...), custom_call_target="tpu_custom_call" | custom-call | tf_op jit(solution)/shard_map/pallas_call | solution.py:170
  60.4 61.0 %shard_map.177 = (bf16[960,128]{1,0:T(8,128)(2,1)}, bf16[960,256]{1,0:T(8,128)(2,1)}, f32[960,128]{1,0:T(8,128)}) custom-call(bf16[960,128]{1,0:T(8,128)(2,1)} %get-tuple-element.14.refs_0_, bf16[128,2048]{1,0:T(8,128)(2,1)} %refs_1_.2, bf16[960,128]{1,0:T(8,128)(2,1)} %fusion.8.refs_0_.refs_2_, f32[1,2048]{1,0:T(1,128)} %bitcast.29, ...), custom_call_target="tpu_custom_call" | custom-call | tf_op jit(solution)/shard_map/pallas_call | solution.py:464
  121.5 0.0 copy-start
  121.5 10.0 %shard_map.178 = (bf16[960,128]{1,0:T(8,128)(2,1)}, f32[96,64,128]{2,1,0:T(8,128)}) custom-call(f32[96]{0:T(128)} %get-tuple-element.40.refs_0_, f32[1536,3]{1,0:T(8,128)} %copy.36.refs_1_, s32[1,1536]{1,0:T(1,128)} %select_n.54.refs_2_, f32[128,128]{1,0:T(8,128)} %exponential_select_fusion.refs_3_, bf16[960,256]{1,0:T(8,128)(2,1)} %get-tuple-element.15.refs_4_, ...), custom_call_target="tpu_custom_call" | custom-call | tf_op jit(solution)/shard_map/pallas_call | solution.py:170
  131.5 30.7 %shard_map.179 = bf16[960,128]{1,0:T(8,128)(2,1)} custom-call(bf16[960,128]{1,0:T(8,128)(2,1)} %get-tuple-element.17.refs_0_, bf16[128,2048]{1,0:T(8,128)(2,1)} %refs_1_.3, bf16[960,128]{1,0:T(8,128)(2,1)} %get-tuple-element.18.refs_2_), custom_call_target="tpu_custom_call" | custom-call | tf_op jit(solution)/shard_map/pallas_call | solution.py:464
  162.2 0.0 copy-done
  162.2 3.6 %fusion.7 = bf16[1536,128]{1,0:T(8,128)(2,1)} fusion(bf16[1536,128]{1,0:T(8,128)(2,1)S(1)} %copy-done, bf16[960,128]{1,0:T(8,128)(2,1)} %shard_map.179, s32[1536]{0:T(1024)S(1)} %broadcast_select_fusion.1, pred[1536]{0:T(1024)(128)(4,1)S(1)} %lt.42), kind=kOutput, calls=%fused_computation.8 | convolution fusion | flops 379355136 | bytes 1039872 | tf_op jit(solution)/shard_map/dot_general | solution.py:531
  (9 shorter events, 0.1 us)
Async XLA Ops:
  121.5 40.7 %copy-start = (bf16[1536,128]{1,0:T(8,128)(2,1)S(1)}, bf16[1536,128]{1,0:T(8,128)(2,1)}, u32[]{:S(2)}) copy-start(bf16[1536,128]{1,0:T(8,128)(2,1)} %param.16) | copy-start | bytes 1179652
